TPU v7x, 32 devices: a whole 2x2x4 slice. The times are simulated.
32 devices in a mesh: sp: 8 (over z, core), tp: 4 (over y, x).
Axes of the slice: x: 2, y: 2, z: 4, core: 2. Of those that a mesh axis runs over, the one named last changes fastest.
Arguments:
- residual_in: bfloat16 [2048, 2048], P('sp'), may hold values from -6 to 6
- queries: bfloat16 [2048, 2048], P('sp', 'tp'), may hold values from -6 to 4
- keys: bfloat16 [2048, 2048], P('sp', 'tp'), may hold values from -4 to 5.2
- values: bfloat16 [2048, 2048], P('sp', 'tp'), may hold values from -9.5 to 9.5
- out_weight: bfloat16 [2048, 2048], P('tp'), may hold values from -0.125 to 0.125
- norm_gain: float32 [2048], replicated, may hold values from 0.1 to 1.9
- expert_routes: int32 [2048, 2], P('sp'), may hold values from 0 to 7, all different within a row; in each aligned block of 256 rows (0 to 255, 256 to 511, ...) at most 128 rows name the same one
- route_scores: float32 [2048, 2], P('sp'), may hold values from -6 to 6
- gate_weight: bfloat16 [8, 2048, 4096], P('sp', None, 'tp'), may hold values from -0.125 to 0.125
- up_weight: bfloat16 [8, 2048, 4096], P('sp', None, 'tp'), may hold values from -0.125 to 0.125
- down_weight: bfloat16 [8, 4096, 2048], P('sp', 'tp'), may hold values from -0.09375 to 0.09375
Outputs:
- layer_out: bfloat16 [2048, 2048], P('sp', 'tp')
Inputs may be any that keep to these rules, and one draw needn't show every extreme that they name: `expert_routes`: each row names 2 different experts; among the 256 rows of one index of sp no expert is named more than 128 times, and in every draw some such block names some expert exactly 128 times.
All inputs are finite; a program needn't handle non-finite values.
Results may differ from a plain program's by a relative error of at most 0.015.
Values may be sent and summed in bfloat16 or wider, within the bound.
A program may use at most 64 MiB of HBM per device.

v0:
```python
import jax
import jax.numpy as jnp
from jax import lax
from jax.sharding import PartitionSpec as P

HD = 64
epsilon = 1e-06


def attend(queries, query_start, keys_all, values_all):
    row_count = queries.shape[0]
    total_len = keys_all.shape[0]
    head_count = queries.shape[1] // HD
    span = min(512, total_len)
    scale = HD ** (-0.5)
    query_heads = queries.reshape(row_count, head_count, HD)
    query_pos = query_start + lax.iota(jnp.int32, row_count)
    block_count = (query_start + row_count - 1 + span - 1) // span

    def one_block(step_index, state_pair):
        accumulated, kept_log = state_pair
        key_start = (block_count - 1 - step_index) * span
        key_block = lax.dynamic_slice_in_dim(keys_all, key_start, span, 0).reshape(
            span, head_count, HD
        )
        value_block = lax.dynamic_slice_in_dim(values_all, key_start, span, 0).reshape(
            span, head_count, HD
        )
        scores = (
            jnp.einsum("qhc,khc->hqk", query_heads, key_block, preferred_element_type=jnp.float32)
            * scale
        )
        key_pos = key_start + lax.iota(jnp.int32, span)
        causal = key_pos[None, :] < query_pos[:, None]
        log_keep = jnp.where(causal, jax.nn.log_sigmoid(-scores), 0.0)
        between = lax.cumsum(log_keep, axis=2, reverse=True) - log_keep + kept_log[:, :, None]
        weights = jnp.where(causal, jnp.exp(jax.nn.log_sigmoid(scores) + between), 0.0).astype(
            jnp.bfloat16
        )
        accumulated = accumulated + jnp.einsum(
            "hqk,khc->qhc", weights, value_block, preferred_element_type=jnp.float32
        )
        return (accumulated, kept_log + jnp.sum(log_keep, axis=2))

    start_pair = (
        jnp.zeros((row_count, head_count, HD), jnp.float32),
        jnp.zeros((head_count, row_count), jnp.float32),
    )
    accumulated, kept_log = lax.fori_loop(0, block_count, one_block, start_pair)
    return accumulated.reshape(row_count, head_count * HD).astype(jnp.bfloat16)


def route_targets(routes, experts, capacity):
    flat_routes = routes.reshape(-1)
    onehot = (flat_routes[:, None] == lax.iota(jnp.int32, experts)[None, :]).astype(jnp.int32)
    before = jnp.cumsum(onehot, axis=0) - onehot
    return flat_routes * capacity + jnp.sum(before * onehot, axis=1)


def shards(
    residual_in,
    queries,
    keys,
    values,
    out_weight,
    norm_gain,
    expert_routes,
    route_scores,
    gate_weight,
    up_weight,
    down_weight,
):
    row_count = residual_in.shape[0]
    width = residual_in.shape[1]
    row_start = lax.axis_index("sp") * row_count
    keys_all, values_all = (
        lax.all_gather(keys, "sp", axis=0, tiled=True),
        lax.all_gather(values, "sp", axis=0, tiled=True),
    )
    mixed_heads = attend(queries, row_start, keys_all, values_all)
    partial_value = jnp.dot(mixed_heads, out_weight, preferred_element_type=jnp.float32).astype(
        jnp.bfloat16
    )
    attended = lax.psum(partial_value, "tp").astype(jnp.float32).astype(jnp.bfloat16)
    stream = (residual_in.astype(jnp.float32) + attended.astype(jnp.float32)).astype(jnp.bfloat16)
    stream_wide = stream.astype(jnp.float32)
    normed = (
        stream_wide
        * lax.rsqrt(jnp.mean(stream_wide * stream_wide, axis=1, keepdims=True) + epsilon)
        * norm_gain
    ).astype(jnp.bfloat16)
    experts = lax.axis_size("sp")
    capacity = 4 * row_count // experts
    top_count = expert_routes.shape[1]
    targets = route_targets(expert_routes, experts, capacity)
    owners = lax.iota(jnp.int32, row_count * top_count) // top_count
    slot_owner = jnp.full((experts * capacity,), row_count, jnp.int32).at[targets].set(owners)
    padded = jnp.concatenate([normed, jnp.zeros((1, width), jnp.bfloat16)], axis=0)
    outgoing = padded[slot_owner].reshape(experts, capacity, width)
    col_count = width // lax.axis_size("tp")
    column_start = lax.axis_index("tp") * col_count
    own_part = lax.dynamic_slice_in_dim(outgoing, column_start, col_count, 2)
    arrived = lax.all_to_all(own_part, "sp", split_axis=0, concat_axis=0, tiled=True)
    arrived = lax.all_gather(arrived, "tp", axis=2, tiled=True)
    slot_rows = arrived.reshape(-1, width)
    gate_act = jnp.dot(slot_rows, gate_weight[0], preferred_element_type=jnp.float32)
    up_act = jnp.dot(slot_rows, up_weight[0], preferred_element_type=jnp.float32)
    hidden = (jax.nn.silu(gate_act) * up_act).astype(jnp.bfloat16)
    expert_part = (
        jnp.dot(hidden, down_weight[0], preferred_element_type=jnp.float32)
        .astype(jnp.bfloat16)
        .reshape(arrived.shape)
    )
    summed = (
        lax.psum_scatter(expert_part, "tp", scatter_dimension=2, tiled=True)
        .astype(jnp.float32)
        .astype(jnp.bfloat16)
    )
    returned = lax.all_to_all(summed, "sp", split_axis=0, concat_axis=0, tiled=True)
    results = returned.reshape(experts * capacity, col_count)
    picked = results[targets].astype(jnp.float32).reshape(row_count, top_count, col_count)
    shares = jax.nn.sigmoid(route_scores - route_scores[:, ::-1])
    combined = jnp.sum(picked * shares[:, :, None], axis=1)
    own_columns = lax.dynamic_slice_in_dim(stream_wide, column_start, col_count, 1)
    return (own_columns + combined).astype(jnp.bfloat16)


def solution(mesh):
    in_specs = (
        P("sp", None),
        P("sp", "tp"),
        P("sp", "tp"),
        P("sp", "tp"),
        P("tp", None),
        P(),
        P("sp", None),
        P("sp", None),
        P("sp", None, "tp"),
        P("sp", None, "tp"),
        P("sp", "tp", None),
    )
    out_specs = P("sp", "tp")
    return jax.shard_map(shards, mesh=mesh, in_specs=in_specs, out_specs=out_specs, check_vma=False)
```

profile of v0, /device:TPU:0, one launch (start us, length us, event | category | flops | bytes accessed | tf_op | source)
XLA Modules:
  0.0 431.7 jit_solution(17356037483601882176)
XLA Ops:
  6.5 0.0 copy-start
  6.5 0.0 all-gather.4.cloned.1.call-start
  6.5 1.9 copy.22
  8.5 0.0 all-gather.4.cloned.1.call-update
  8.5 0.0 all-gather.6.cloned.1.call-start
  8.6 1.8 copy.23
  10.3 0.0 all-gather.6.cloned.1.call-update
  10.4 0.0 all-reduce.3.cloned.1.call-start
  10.4 1.1 copy.24
  11.5 30.8 %all-gather.4.cloned.1.call-done = bf16[2048,512]{0,1:T(8,128)(2,1)} async-done(((bf16[256,512]{0,1:T(8,128)(2,1)}), bf16[2048,512]{0,1:T(8,128)(2,1)}) %all-gather.4.cloned.1.call-update) | async-done | bytes 2097168 | tf_op jit(solution)/shard_map/all_gather | solution.py:78
  42.3 31.2 %all-gather.6.cloned.1.call-done = bf16[2048,512]{0,1:T(8,128)(2,1)} async-done(((bf16[256,512]{0,1:T(8,128)(2,1)}), bf16[2048,512]{0,1:T(8,128)(2,1)}) %all-gather.6.cloned.1.call-update) | async-done | bytes 2097168 | tf_op jit(solution)/shard_map/all_gather | solution.py:77
  73.6 23.8 %while.15 = (s32[]{:T(128)}, f32[256,8,64]{0,2,1:T(8,128)S(1)}, f32[8,256]{1,0:T(8,128)S(1)}, s32[]{:T(128)}, s32[]{:T(128)}, /*index=5*/bf16[2048,512]{0,1:T(8,...) while((s32[]{:T(128)}, f32[256,8,64]{0,2,1:T(8,128)S(1)}, ...), condition=%wide.region_4.5_spmd.clone, body=%wide.region_0.4_spmd.clone.sunk | while | flops 436501248 | bytes 51206344 | solution.py:49
  73.6 1.3 constant_dynamic-slice_fusion.4
  74.9 0.1 broadcast_compare_fusion.2
  75.1 3.6 fusion.64
  78.7 10.1 %fusion.65 = f32[8,256,4,128]{1,0,3,2:T(8,128)S(1)} fusion(f32[8,256,4,128]{1,3,2,0:T(8,128)S(1)} %bitcast.101), kind=kOutput, calls=%fused_computation.22.clone.1 | output fusion | flops 133169152 | bytes 8388608 | tf_op jit(solution)/shard_map/reduce-window.6
  88.8 0.1 fusion.66
  88.9 0.3 broadcast_add_fusion.2
  89.2 1.4 copy.35
  90.6 6.3 %fusion.67 = bf16[8,256,512]{1,2,0:T(8,128)(2,1)S(1)} fusion(f32[8,256,4,128]{1,3,2,0:T(8,128)S(1)} %copy.35, f32[8,512,256]{2,1,0:T(8,128)S(1)} %get-tuple-element.219, f32[8,256]{1,0:T(8,128)S(1)} %get-tuple-element.236, pred[256,512]{0,1:T(8,128)(4,1)S(1)} %broadcast_compare_fusion.2), kind=kLoop, calls=%fused_computation.10.clone.1 | loop fusion | flops 23068672 | bytes 10625024 | tf_op jit(solution)/shard_map/while/body/convert_element_type | solution.py:37
  96.9 0.5 fusion.68
  97.4 0.0 copy-start.4
  97.5 0.0 copy-start.1
  97.5 0.0 copy-done
  97.5 0.0 copy-start.3
  97.5 1.8 convolution_convert_fusion
  99.3 0.0 all-reduce.3.cloned.1.call-update
  99.3 0.0 all-gather.8.cloned.1.call-start
  99.4 0.0 copy-done.4
  99.4 0.1 copy.26
  99.5 0.1 eq.29
  99.7 0.1 eq.25
  99.8 0.1 copy.25
  100.0 0.1 mul.81
  100.1 1.1 reduce-window.24
  101.3 0.2 slice_reduce_fusion
  101.5 0.1 fusion.32
  101.6 2.6 scatter_custom_fusion
  104.3 117.7 %all-reduce.3.cloned.1.call-done = bf16[256,2048]{1,0:T(8,128)(2,1)} async-done(((bf16[256,2048]{1,0:T(8,128)(2,1)}), bf16[256,2048]{1,0:T(8,128)(2,1)}) %all-reduce.3.cloned.1.call-update) | async-done | bytes 1048592 | tf_op jit(solution)/shard_map/psum | solution.py:84
  222.0 0.0 copy-done.1
  222.0 3.0 fusion.30
  225.0 0.0 copy-done.2
  225.0 0.5 multiply_convert_fusion.1
  225.5 0.1 concatenate.3
  225.6 6.0 %gather_fusion = bf16[1024,2048]{1,0:T(8,128)(2,1)} fusion(bf16[257,2048]{1,0:T(8,128)(2,1)S(1)} %concatenate.3, s32[1024]{0:T(1024)S(1)} %fusion.34), kind=kCustom, calls=%fused_computation | custom fusion | bytes 8392704 | tf_op jit(solution)/shard_map/gather | solution.py:99
  231.6 1.3 constant_dynamic-slice_fusion.2
  233.0 31.1 %all_to_all.10 = bf16[8,128,512]{2,1,0:T(8,128)(2,1)} all-to-all(bf16[8,128,512]{2,1,0:T(8,128)(2,1)S(1)} %constant_dynamic-slice_fusion.2), channel_id=1, replica_groups=mesh['sp'=8,'tp'=4] {'sp'}, dimensions={0} | all-to-all | bytes 2097152 | tf_op jit(solution)/shard_map/all_to_all | solution.py:103
  264.0 0.0 all-gather.8.cloned.1.call-update
  264.1 0.0 reduce-scatter.2.cloned.1.call-start
  264.1 50.5 %all-gather.8.cloned.1.call-done = bf16[8,128,2048]{2,1,0:T(8,128)(2,1)} async-done(((bf16[8,128,512]{2,1,0:T(8,128)(2,1)}), bf16[8,128,2048]{2,1,0:T(8,128)(2,1)}) %all-gather.8.cloned.1.call-update) | async-done | bytes 4194320 | tf_op jit(solution)/shard_map/all_gather | solution.py:104
  314.6 7.6 %fusion.21 = f32[1024,1024]{1,0:T(8,128)S(1)} fusion(bf16[1024,2048]{1,0:T(8,128)(2,1)} %bitcast.112, bf16[1,2048,1024]{2,1,0:T(8,128)(2,1)} %param.22), kind=kOutput, calls=%fused_computation.37 | convolution fusion | flops 4294967296 | bytes 12582912 | tf_op jit(solution)/shard_map/dot_general | solution.py:107
  322.3 0.0 copy-start.7
  322.3 5.4 %multiply_convert_fusion = bf16[1024,1024]{1,0:T(8,128)(2,1)S(1)} fusion(f32[1024,1024]{1,0:T(8,128)S(1)} %fusion.21, bf16[1024,2048]{1,0:T(8,128)(2,1)S(1)} %bitcast.113, bf16[1,2048,1024]{2,1,0:T(8,128)(2,1)S(1)} %copy-done.6), kind=kOutput, calls=%fused_computation.41 | convolution fusion | flops 4301258752 | bytes 14680064 | tf_op jit(solution)/shard_map/dot_general | solution.py:106
  327.7 6.1 %fusion.25 = bf16[1024,2048]{1,0:T(8,128)(2,1)} fusion(bf16[1024,1024]{1,0:T(8,128)(2,1)S(1)} %multiply_convert_fusion, bf16[1,1024,2048]{2,1,0:T(8,128)(2,1)S(1)} %copy-done.7), kind=kOutput, calls=%fused_computation.42 | convolution fusion | flops 4297064448 | bytes 10485760 | tf_op jit(solution)/shard_map/dot_general | solution.py:110
  333.7 0.0 reduce-scatter.2.cloned.1.call-update
  333.8 52.7 %reduce-scatter.2.cloned.1.call-done = bf16[8,128,512]{2,1,0:T(8,128)(2,1)} async-done(((bf16[8,128,2048]{2,1,0:T(8,128)(2,1)}), bf16[8,128,512]{2,1,0:T(8,128)(2,1)}) %reduce-scatter.2.cloned.1.call-update) | async-done | bytes 1048592 | tf_op jit(solution)/shard_map/reduce_scatter | solution.py:115
  386.5 4.6 %all-to-all-start.1 = ((bf16[8,128,512]{2,1,0:T(8,128)(2,1)}), bf16[8,128,512]{2,1,0:T(8,128)(2,1)S(1)}, u32[]{:S(2)}, u32[]{:S(2)}) async-start(bf16[8,128,512]{2,1,0:T(8,128)(2,1)} %reduce-scatter.2.cloned.1.call-done), calls=%async_computation.2 | async-start | bytes 2097152 | tf_op jit(solution)/shard_map/all_to_all | solution.py:119
  391.1 0.1 rev.3
  391.2 0.1 copy.28
  391.4 26.3 %all-to-all-done.1 = bf16[8,128,512]{2,1,0:T(8,128)(2,1)S(1)} async-done(((bf16[8,128,512]{2,1,0:T(8,128)(2,1)}), bf16[8,128,512]{2,1,0:T(8,128)(2,1)S(1)}, u32[]{:S(2)}, u32[]{:S(2)}) %all-to-all-start.1) | async-done | bytes 1048608 | tf_op jit(solution)/shard_map/all_to_all | solution.py:119
  417.7 2.6 gather_fusion.1
  420.3 1.7 reshape.117
  422.0 1.3 multiply_reduce_fusion.1
  423.3 1.8 add_convert_fusion.1
  (26 shorter events, 0.2 us)
Async XLA Ops:
  6.5 91.0 %copy-start = (bf16[512,2048]{1,0:T(8,128)(2,1)S(1)}, bf16[512,2048]{1,0:T(8,128)(2,1)}, u32[]{:S(2)}) copy-start(bf16[512,2048]{1,0:T(8,128)(2,1)} %param.17) | copy-start | bytes 6291460
  6.5 35.8 %all-gather.4.cloned.1.call-start = ((), (), s32[]{:S(2)}) async-start(), calls=%async_computation.3 | async-start | bytes 2359296 | tf_op jit(solution)/shard_map/all_gather | solution.py:78
  8.5 65.0 %all-gather.6.cloned.1.call-start = ((), (), s32[]{:S(2)}) async-start(), calls=%async_computation.4 | async-start | bytes 2359296 | tf_op jit(solution)/shard_map/all_gather | solution.py:77
  10.4 211.6 %all-reduce.3.cloned.1.call-start = ((), (), s32[]{:S(2)}) async-start(), calls=%async_computation.5 | async-start | bytes 2097152 | tf_op jit(solution)/shard_map/psum | solution.py:84
  97.4 1.9 copy-start.4
  97.5 124.5 %copy-start.1 = (bf16[256,2048]{1,0:T(8,128)(2,1)S(1)}, bf16[256,2048]{1,0:T(8,128)(2,1)}, u32[]{:S(2)}) copy-start(bf16[256,2048]{1,0:T(8,128)(2,1)} %param.13) | copy-start | bytes 3145732
  97.5 127.5 %copy-start.3 = (f32[2048]{0:T(1024)S(1)}, f32[2048]{0:T(1024)}, u32[]{:S(2)}) copy-start(f32[2048]{0:T(1024)} %param.18) | copy-start | bytes 24580
  99.3 215.3 %all-gather.8.cloned.1.call-start = ((), (), s32[]{:S(2)}) async-start(), calls=%async_computation.6 | async-start | bytes 5242880 | tf_op jit(solution)/shard_map/all_gather | solution.py:104
  222.0 3.0 copy-start.2
  264.1 122.4 %reduce-scatter.2.cloned.1.call-start = ((), (), s32[]{:S(2)}) async-start(), calls=%async_computation.7 | async-start | bytes 5242880 | tf_op jit(solution)/shard_map/reduce_scatter | solution.py:115
  314.6 7.7 %copy-start.6 = (bf16[1,2048,1024]{2,1,0:T(8,128)(2,1)S(1)}, bf16[1,2048,1024]{2,1,0:T(8,128)(2,1)}, u32[]{:S(2)}) copy-start(bf16[1,2048,1024]{2,1,0:T(8,128)(2,1)} %param.21) | copy-start | bytes 12582916
  314.6 7.7 %copy-start.8 = (bf16[8,128,2048]{2,1,0:T(8,128)(2,1)S(1)}, bf16[8,128,2048]{2,1,0:T(8,128)(2,1)}, u32[]{:S(2)}) copy-start(bf16[8,128,2048]{2,1,0:T(8,128)(2,1)} %all-gather.8.cloned.1.call-done) | copy-start | bytes 12582916
  322.3 5.4 %copy-start.7 = (bf16[1,1024,2048]{2,1,0:T(8,128)(2,1)S(1)}, bf16[1,1024,2048]{2,1,0:T(8,128)(2,1)}, u32[]{:S(2)}) copy-start(bf16[1,1024,2048]{2,1,0:T(8,128)(2,1)} %param.23) | copy-start | bytes 12582916
  333.7 57.4 %copy-start.5 = (f32[256,2]{0,1:T(2,128)S(1)}, f32[256,2]{0,1:T(2,128)}, u32[]{:S(2)}) copy-start(f32[256,2]{0,1:T(2,128)} %param.20) | copy-start | bytes 6148
  386.5 31.2 %all-to-all-start.1 = ((bf16[8,128,512]{2,1,0:T(8,128)(2,1)}), bf16[8,128,512]{2,1,0:T(8,128)(2,1)S(1)}, u32[]{:S(2)}, u32[]{:S(2)}) async-start(bf16[8,128,512]{2,1,0:T(8,128)(2,1)} %reduce-scatter.2.cloned.1.call-done), calls=%async_computation.2 | async-start | bytes 2097152 | tf_op jit(solution)/shard_map/all_to_all | solution.py:119
Sparse Core Ops, SparseCore 0:
  8.9 33.3 all-gather.3
  43.9 29.6 all-gather.5
  99.4 122.5 all-reduce.2
  264.2 50.3 all-gather.7
  333.9 52.5 reduce-scatter.1
where the time goes:
time: 432 us
  waiting for transfers between devices  309 us (72%)
  blocking collectives  31.1 us (7%)
  matrix products  25 us (6%)
  other arithmetic  24.9 us (6%)
  local copies, waits for them, and re-layouts  23 us (5%)
  between operations  13.4 us (3%)
  starting transfers between devices  4.78 us (1%)
    psum x1, waiting for transfers between devices, shards(): lax.psum(partial_value, 'tp').astype(jnp.float32).astype(jnp.bfloat16)  118 us
    reduce_scatter x1, waiting for transfers between devices, shards(): lax.psum_scatter(expert_part, 'tp', scatter_dimension=2, tiled=True)  52.7 us
    all_gather x1, waiting for transfers between devices, shards(): arrived = lax.all_gather(arrived, 'tp', axis=2, tiled=True)  50.5 us
    all_gather x1, waiting for transfers between devices, shards(): lax.all_gather(keys, 'sp', axis=0, tiled=True)  31.2 us
    all_to_all x1, blocking collectives, shards(): lax.all_to_all(own_part, 'sp', split_axis=0, concat_axis=0, tiled=True)  31.1 us
    all_gather x1, waiting for transfers between devices, shards(): lax.all_gather(values, 'sp', axis=0, tiled=True)  30.8 us
    all_to_all x1, waiting for transfers between devices, shards(): lax.all_to_all(summed, 'sp', split_axis=0, concat_axis=0, tiled=True)  26.3 us
    another operation x4, other arithmetic  11.3 us
  transfers between devices with their start and end apart: 6, of which 6 were waited for; matrix products, arithmetic and copies ran while one was open for 2% of the time, Pallas kernels for 0%

commit v1 on v0

--- a/solution.py
+++ b/solution.py
@@ -101,7 +101,8 @@
     column_start = lax.axis_index("tp") * col_count
     own_part = lax.dynamic_slice_in_dim(outgoing, column_start, col_count, 2)
     arrived = lax.all_to_all(own_part, "sp", split_axis=0, concat_axis=0, tiled=True)
-    arrived = lax.all_gather(arrived, "tp", axis=2, tiled=True)
+    pieces = lax.all_gather(arrived, "tp", axis=0, tiled=False)
+    arrived = jnp.concatenate(pieces, axis=2)
     slot_rows = arrived.reshape(-1, width)
     gate_act = jnp.dot(slot_rows, gate_weight[0], preferred_element_type=jnp.float32)
     up_act = jnp.dot(slot_rows, up_weight[0], preferred_element_type=jnp.float32)

time: 432 us -> 447 us (1.035)
  local copies, waits for them, and re-layouts: 23 us -> 30.5 us
  matrix products: 25 us -> 32.2 us
    dot_general x1, matrix products: 6.07 us -> 16.3 us  [shards(): jnp.dot(hidden, down_weight[0], preferred_element_type=jnp.float32)]
    reshape x0 -> x1, local copies, waits for them, and re-layouts: none -> 7.51 us  [shards(): arrived = jnp.concatenate(pieces, axis=2)]
    dot_general x1 -> x0, matrix products: 5.35 us -> none  [shards(): jnp.dot(slot_rows, gate_weight[0], preferred_element_type=jnp.float32)]
where the time goes in v1:
time: 447 us
  waiting for transfers between devices  310 us (69%)
  matrix products  32.2 us (7%)
  blocking collectives  31.1 us (7%)
  local copies, waits for them, and re-layouts  30.5 us (7%)
  other arithmetic  24.9 us (6%)
  between operations  13.4 us (3%)
  starting transfers between devices  4.78 us (1%)
    psum x1, waiting for transfers between devices, shards(): lax.psum(partial_value, 'tp').astype(jnp.float32).astype(jnp.bfloat16)  118 us
    reduce_scatter x1, waiting for transfers between devices, shards(): lax.psum_scatter(expert_part, 'tp', scatter_dimension=2, tiled=True)  52.8 us
    all_gather x1, waiting for transfers between devices, shards(): pieces = lax.all_gather(arrived, 'tp', axis=0, tiled=False)  50.6 us
    all_gather x1, waiting for transfers between devices, shards(): lax.all_gather(keys, 'sp', axis=0, tiled=True)  31.2 us
    all_to_all x1, blocking collectives, shards(): lax.all_to_all(own_part, 'sp', split_axis=0, concat_axis=0, tiled=True)  31.1 us
    all_gather x1, waiting for transfers between devices, shards(): lax.all_gather(values, 'sp', axis=0, tiled=True)  30.8 us
    all_to_all x1, waiting for transfers between devices, shards(): lax.all_to_all(summed, 'sp', split_axis=0, concat_axis=0, tiled=True)  26.3 us
    dot_general x1, matrix products, shards(): jnp.dot(hidden, down_weight[0], preferred_element_type=jnp.float32)  16.3 us
  transfers between devices with their start and end apart: 6, of which 6 were waited for; matrix products, arithmetic and copies ran while one was open for 2% of the time, Pallas kernels for 0%

profile of v1, /device:TPU:0, one launch (start us, length us, event | category | flops | bytes accessed | tf_op | source)
XLA Modules:
  0.0 446.6 jit_solution(4780756000065381146)
XLA Ops:
  6.5 0.0 copy-start
  6.5 0.0 all-gather.5.cloned.1.call-start
  6.5 1.9 copy.43
  8.5 0.0 all-gather.5.cloned.1.call-update
  8.5 0.0 all-gather.7.cloned.1.call-start
  8.6 1.8 copy.44
  10.3 0.0 all-gather.7.cloned.1.call-update
  10.4 0.0 all-reduce.3.cloned.1.call-start
  10.4 1.1 copy.45
  11.5 30.8 %all-gather.5.cloned.1.call-done = bf16[2048,512]{0,1:T(8,128)(2,1)} async-done(((bf16[256,512]{0,1:T(8,128)(2,1)}), bf16[2048,512]{0,1:T(8,128)(2,1)}) %all-gather.5.cloned.1.call-update) | async-done | bytes 2097168 | tf_op jit(solution)/shard_map/all_gather | solution.py:78
  42.3 31.2 %all-gather.7.cloned.1.call-done = bf16[2048,512]{0,1:T(8,128)(2,1)} async-done(((bf16[256,512]{0,1:T(8,128)(2,1)}), bf16[2048,512]{0,1:T(8,128)(2,1)}) %all-gather.7.cloned.1.call-update) | async-done | bytes 2097168 | tf_op jit(solution)/shard_map/all_gather | solution.py:77
  73.6 23.8 %while.15 = (s32[]{:T(128)}, f32[256,8,64]{0,2,1:T(8,128)S(1)}, f32[8,256]{1,0:T(8,128)S(1)}, s32[]{:T(128)}, s32[]{:T(128)}, /*index=5*/bf16[2048,512]{0,1:T(8,...) while((s32[]{:T(128)}, f32[256,8,64]{0,2,1:T(8,128)S(1)}, ...), condition=%wide.region_4.5_spmd.clone, body=%wide.region_0.4_spmd.clone.sunk | while | flops 436501248 | bytes 51206344 | solution.py:49
  73.6 1.3 constant_dynamic-slice_fusion.4
  74.9 0.1 broadcast_compare_fusion.2
  75.1 3.6 fusion.73
  78.7 10.1 %fusion.74 = f32[8,256,4,128]{1,0,3,2:T(8,128)S(1)} fusion(f32[8,256,4,128]{1,3,2,0:T(8,128)S(1)} %bitcast.115), kind=kOutput, calls=%fused_computation.22.clone.1 | output fusion | flops 133169152 | bytes 8388608 | tf_op jit(solution)/shard_map/reduce-window.6
  88.8 0.1 fusion.75
  88.9 0.3 broadcast_add_fusion.2
  89.2 1.4 copy.70
  90.6 6.3 %fusion.76 = bf16[8,256,512]{1,2,0:T(8,128)(2,1)S(1)} fusion(f32[8,256,4,128]{1,3,2,0:T(8,128)S(1)} %copy.70, f32[8,512,256]{2,1,0:T(8,128)S(1)} %get-tuple-element.219, f32[8,256]{1,0:T(8,128)S(1)} %get-tuple-element.236, pred[256,512]{0,1:T(8,128)(4,1)S(1)} %broadcast_compare_fusion.2), kind=kLoop, calls=%fused_computation.10.clone.1 | loop fusion | flops 23068672 | bytes 10625024 | tf_op jit(solution)/shard_map/while/body/convert_element_type | solution.py:37
  96.9 0.5 fusion.77
  97.4 0.0 copy-start.4
  97.5 0.0 copy-start.1
  97.5 0.0 copy-done
  97.5 0.0 copy-start.3
  97.5 1.8 convolution_convert_fusion
  99.3 0.0 all-reduce.3.cloned.1.call-update
  99.3 0.0 all-gather.9.cloned.1.call-start
  99.4 0.0 copy-done.4
  99.4 0.1 copy.47
  99.5 0.1 eq.29
  99.7 0.1 eq.25
  99.8 0.1 copy.46
  100.0 0.1 mul.81
  100.1 1.1 reduce-window.24
  101.3 0.2 slice_reduce_fusion
  101.5 0.1 fusion.43
  101.6 2.6 scatter_custom_fusion
  104.3 117.7 %all-reduce.3.cloned.1.call-done = bf16[256,2048]{1,0:T(8,128)(2,1)} async-done(((bf16[256,2048]{1,0:T(8,128)(2,1)}), bf16[256,2048]{1,0:T(8,128)(2,1)}) %all-reduce.3.cloned.1.call-update) | async-done | bytes 1048592 | tf_op jit(solution)/shard_map/psum | solution.py:84
  222.0 0.0 copy-done.1
  222.0 3.0 fusion.41
  225.0 0.0 copy-done.3
  225.0 0.0 copy-done.2
  225.0 0.5 multiply_convert_fusion.2
  225.5 0.1 concatenate.3
  225.6 6.0 %gather_fusion = bf16[1024,2048]{1,0:T(8,128)(2,1)} fusion(bf16[257,2048]{1,0:T(8,128)(2,1)S(1)} %concatenate.3, s32[1024]{0:T(1024)S(1)} %fusion.45), kind=kCustom, calls=%fused_computation | custom fusion | bytes 8392704 | tf_op jit(solution)/shard_map/gather | solution.py:99
  231.7 1.3 constant_dynamic-slice_fusion.2
  233.0 31.1 %all_to_all.10 = bf16[8,128,512]{2,1,0:T(8,128)(2,1)} all-to-all(bf16[8,128,512]{2,1,0:T(8,128)(2,1)S(1)} %constant_dynamic-slice_fusion.2), channel_id=1, replica_groups=mesh['sp'=8,'tp'=4] {'sp'}, dimensions={0} | all-to-all | bytes 2097152 | tf_op jit(solution)/shard_map/all_to_all | solution.py:103
  264.1 0.0 all-gather.9.cloned.1.call-update
  264.1 0.0 reduce-scatter.2.cloned.1.call-start
  264.1 50.6 %all-gather.9.cloned.1.call-done = bf16[32,128,512]{2,1,0:T(8,128)(2,1)} async-done(((bf16[8,128,512]{2,1,0:T(8,128)(2,1)}), bf16[32,128,512]{2,1,0:T(8,128)(2,1)}) %all-gather.9.cloned.1.call-update) | async-done | bytes 4194320 | tf_op jit(solution)/shard_map/all_gather | solution.py:104
  314.8 7.5 %copy.49 = bf16[8,128,4,512]{1,0,3,2:T(8,128)(2,1)} copy(bf16[8,128,4,512]{3,1,0,2:T(8,128)(2,1)} %bitcast.120) | data formatting | bytes 8388608 | tf_op jit(solution)/shard_map/reshape | solution.py:105
  322.3 10.0 %fusion.19 = f32[1024,1024]{1,0:T(8,128)} fusion(bf16[1,2048,1024]{2,1,0:T(8,128)(2,1)} %param.22, bf16[256,8,8,128]{3,2,1,0:T(8,128)(2,1)} %bitcast.122), kind=kOutput, calls=%fused_computation.35 | convolution fusion | flops 4294967296 | bytes 12582912 | tf_op jit(solution)/shard_map/dot_general | solution.py:108
  332.3 16.3 %fusion.27 = bf16[1024,2048]{1,0:T(8,128)(2,1)} fusion(bf16[1,1024,2048]{2,1,0:T(8,128)(2,1)} %param.23, f32[1024,1024]{1,0:T(8,128)} %fusion.19, bf16[1,2048,1024]{2,1,0:T(8,128)(2,1)} %param.21, bf16[256,8,8,128]{3,2,1,0:T(8,128)(2,1)} %bitcast.123), kind=kOutput, calls=%fused_computation.44 | convolution fusion | flops 8598323200 | bytes 20971520 | tf_op jit(solution)/shard_map/dot_general | solution.py:111
  348.6 0.0 reduce-scatter.2.cloned.1.call-update
  348.6 52.8 %reduce-scatter.2.cloned.1.call-done = bf16[8,128,512]{2,1,0:T(8,128)(2,1)} async-done(((bf16[8,128,2048]{2,1,0:T(8,128)(2,1)}), bf16[8,128,512]{2,1,0:T(8,128)(2,1)}) %reduce-scatter.2.cloned.1.call-update) | async-done | bytes 1048592 | tf_op jit(solution)/shard_map/reduce_scatter | solution.py:116
  401.4 4.6 %all-to-all-start.1 = ((bf16[8,128,512]{2,1,0:T(8,128)(2,1)}), bf16[8,128,512]{2,1,0:T(8,128)(2,1)S(1)}, u32[]{:S(2)}, u32[]{:S(2)}) async-start(bf16[8,128,512]{2,1,0:T(8,128)(2,1)} %reduce-scatter.2.cloned.1.call-done), calls=%async_computation.2 | async-start | bytes 2097152 | tf_op jit(solution)/shard_map/all_to_all | solution.py:120
  406.0 0.1 rev.3
  406.1 0.1 copy.50
  406.3 26.3 %all-to-all-done.1 = bf16[8,128,512]{2,1,0:T(8,128)(2,1)S(1)} async-done(((bf16[8,128,512]{2,1,0:T(8,128)(2,1)}), bf16[8,128,512]{2,1,0:T(8,128)(2,1)S(1)}, u32[]{:S(2)}, u32[]{:S(2)}) %all-to-all-start.1) | async-done | bytes 1048608 | tf_op jit(solution)/shard_map/all_to_all | solution.py:120
  432.6 2.6 gather_fusion.1
  435.2 1.7 reshape.117
  436.9 1.3 multiply_reduce_fusion.1
  438.2 1.8 add_convert_fusion.1
  (20 shorter events, 0.2 us)
Async XLA Ops:
  6.5 91.0 %copy-start = (bf16[512,2048]{1,0:T(8,128)(2,1)S(1)}, bf16[512,2048]{1,0:T(8,128)(2,1)}, u32[]{:S(2)}) copy-start(bf16[512,2048]{1,0:T(8,128)(2,1)} %param.17) | copy-start | bytes 6291460
  6.5 35.8 %all-gather.5.cloned.1.call-start = ((), (), s32[]{:S(2)}) async-start(), calls=%async_computation.3 | async-start | bytes 2359296 | tf_op jit(solution)/shard_map/all_gather | solution.py:78
  8.5 65.0 %all-gather.7.cloned.1.call-start = ((), (), s32[]{:S(2)}) async-start(), calls=%async_computation.4 | async-start | bytes 2359296 | tf_op jit(solution)/shard_map/all_gather | solution.py:77
  10.4 211.6 %all-reduce.3.cloned.1.call-start = ((), (), s32[]{:S(2)}) async-start(), calls=%async_computation.5 | async-start | bytes 2097152 | tf_op jit(solution)/shard_map/psum | solution.py:84
  97.4 1.9 copy-start.4
  97.5 124.5 %copy-start.1 = (bf16[256,2048]{1,0:T(8,128)(2,1)S(1)}, bf16[256,2048]{1,0:T(8,128)(2,1)}, u32[]{:S(2)}) copy-start(bf16[256,2048]{1,0:T(8,128)(2,1)} %param.13) | copy-start | bytes 3145732
  97.5 127.5 %copy-start.3 = (f32[2048]{0:T(1024)S(1)}, f32[2048]{0:T(1024)}, u32[]{:S(2)}) copy-start(f32[2048]{0:T(1024)} %param.18) | copy-start | bytes 24580
  99.3 215.5 %all-gather.9.cloned.1.call-start = ((), (), s32[]{:S(2)}) async-start(), calls=%async_computation.7 | async-start | bytes 5242880 | tf_op jit(solution)/shard_map/all_gather | solution.py:104
  222.0 3.0 copy-start.2
  264.1 137.3 %reduce-scatter.2.cloned.1.call-start = ((), (), s32[]{:S(2)}) async-start(), calls=%async_computation.6 | async-start | bytes 5242880 | tf_op jit(solution)/shard_map/reduce_scatter | solution.py:116
  348.6 57.4 %copy-start.5 = (f32[256,2]{0,1:T(2,128)S(1)}, f32[256,2]{0,1:T(2,128)}, u32[]{:S(2)}) copy-start(f32[256,2]{0,1:T(2,128)} %param.20) | copy-start | bytes 6148
  401.4 31.2 %all-to-all-start.1 = ((bf16[8,128,512]{2,1,0:T(8,128)(2,1)}), bf16[8,128,512]{2,1,0:T(8,128)(2,1)S(1)}, u32[]{:S(2)}, u32[]{:S(2)}) async-start(bf16[8,128,512]{2,1,0:T(8,128)(2,1)} %reduce-scatter.2.cloned.1.call-done), calls=%async_computation.2 | async-start | bytes 2097152 | tf_op jit(solution)/shard_map/all_to_all | solution.py:120
Sparse Core Ops, SparseCore 0:
  8.9 33.3 all-gather.4
  43.9 29.6 all-gather.6
  99.4 122.5 all-reduce.2
  264.2 50.5 all-gather.8
  348.7 52.5 reduce-scatter.1
